TPU v7x, 512 devices: a whole 4x4x16 slice. The times are simulated.
512 devices in a mesh: sp: 32 (over z, core), tp: 16 (over y, x).
Axes of the slice: x: 4, y: 4, z: 16, core: 2. Of those that a mesh axis runs over, the one named last changes fastest.
Arguments:
- residual_in: bfloat16 [8192, 2048], P(('sp', 'tp')), may hold values from -6 to 6
- query_a: bfloat16 [8192, 1024], P('sp', 'tp'), may hold values from -12 to 12
- key_a: bfloat16 [8192, 1024], P('sp', 'tp'), may hold values from -12 to 12
- value_a: bfloat16 [8192, 1024], P('sp', 'tp'), may hold values from -6 to 6
- query_b: bfloat16 [8192, 2048], P('sp', 'tp'), may hold values from -12 to 12
- key_b: bfloat16 [8192, 2048], P('sp', 'tp'), may hold values from -12 to 12
- value_b: bfloat16 [8192, 2048], P('sp', 'tp'), may hold values from -6 to 6
- cum_gates: float32 [8192, 2, 16], P('sp', None, 'tp'), may hold values from -985.04 to 0, as said below
- out_a: bfloat16 [1024, 2048], P('tp'), may hold values from -0.1875 to 0.1875
- out_b: bfloat16 [2048, 2048], P('tp'), may hold values from -0.125 to 0.125
- post_gain: bfloat16 [2048], replicated, may hold values from 0.099609375 to 1.8984375
- pre_gain: bfloat16 [2048], replicated, may hold values from 0.099609375 to 1.8984375
- expert_ids: int32 [8192, 2], P('sp'), may hold values from 0 to 31, all different within a row; in each aligned block of 256 rows (0 to 255, 256 to 511, ...) at most 20 rows name the same one
- expert_weights: float32 [8192, 2], P('sp'), may hold values from 0.2 to 1
- w_gate: bfloat16 [32, 2048, 4096], P('sp', None, 'tp'), may hold values from -0.125 to 0.125
- w_up: bfloat16 [32, 2048, 4096], P('sp', None, 'tp'), may hold values from -0.125 to 0.125
- w_down: bfloat16 [32, 4096, 2048], P('sp', 'tp'), may hold values from -0.09375 to 0.09375
Outputs:
- layer_out: bfloat16 [8192, 2048], P(('sp', 'tp'))
Inputs may be any that keep to these rules, and one draw needn't show every extreme that they name: `expert_ids`: in each aligned block of 256 positions no expert is named by more than 20 routes, a bound that some block reaches; a token's experts differ. `cum_gates`: never rises along the positions.
All inputs are finite; a program needn't handle non-finite values.
Results may differ from a plain program's by a relative error of at most 0.015.
Values may be sent and summed in bfloat16 or wider, within the bound.
A program may use at most 64 MiB of HBM per device.

v0:
```python
import jax
import jax.numpy as jnp
from jax import lax
from jax.sharding import PartitionSpec as P

eps_norm = 1e-06
big_neg = -1e30


def joined_along(blocks, dim):
    dims = list(blocks.shape[1:])
    dims[dim] *= blocks.shape[0]
    return jnp.moveaxis(blocks, 0, dim).reshape(dims)


def from_everyone(array, axis):
    copies = jnp.broadcast_to(array, (lax.axis_size(axis), *array.shape))
    return lax.all_to_all(copies, axis, split_axis=0, concat_axis=0, tiled=True)


def gathered_copies(array, axis, dim):
    return joined_along(from_everyone(array, axis), dim)


def side_by_side(arrays, axis, dim, along):
    ends, at = ([], 0)
    for a in arrays[:-1]:
        at += a.shape[along]
        ends.append(at)
    both = jnp.concatenate(arrays, axis=along)
    return tuple(jnp.split(lax.all_gather(both, axis, axis=dim, tiled=True), ends, axis=along))


def split_up(array, dim, devices):
    before, after = (array.shape[:dim], array.shape[dim + 1 :])
    return jnp.moveaxis(array.reshape(*before, devices, -1, *after), dim, 0)


def summed_on_arrival(array, axis, dim):
    blocks = split_up(array, dim, lax.axis_size(axis))
    arrived = lax.all_to_all(blocks, axis, split_axis=0, concat_axis=0, tiled=True)
    return arrived.astype(jnp.float32).sum(axis=0)


def rms_scale(values, gain):
    return values * lax.rsqrt(jnp.mean(values * values, axis=-1, keepdims=True) + eps_norm) * gain


def empty_state(item_count, heads, width):
    return (
        jnp.full((heads, item_count), big_neg, jnp.float32),
        jnp.zeros((heads, item_count), jnp.float32),
        jnp.zeros((heads, item_count, width), jnp.float32),
    )


def update_state(state, query, key_rows, values, query_gate, key_gate, mask, width):
    highest, total, accum = state
    score = jnp.einsum(
        "rhd,khd->hrk", query, key_rows, preferred_element_type=jnp.float32
    ) * width ** (-0.5)
    score = score + query_gate.T[:, :, None] - key_gate.T[:, None, :]
    new_high = jnp.maximum(highest, jnp.max(jnp.where(mask[None], score, big_neg), axis=2))
    expo = jnp.exp(jnp.where(mask[None], score - new_high[:, :, None], big_neg))
    total = jnp.sum(expo, axis=2)
    accum = jnp.einsum(
        "hrk,khd->hrd", expo.astype(jnp.bfloat16), values, preferred_element_type=jnp.float32
    )
    return (new_high, total, accum)


def finish(state):
    highest, total, accum = state
    heads, item_count, width = accum.shape
    result = accum / total[:, :, None]
    return result.transpose(1, 0, 2).reshape(item_count, heads * width).astype(jnp.bfloat16)


def per_device(
    residual_in,
    query_a,
    key_a,
    value_a,
    query_b,
    key_b,
    value_b,
    cum_gates,
    out_a,
    out_b,
    post_gain,
    pre_gain,
    expert_ids,
    expert_weights,
    w_gate,
    w_up,
    w_down,
):
    rows = query_a.shape[0]
    heads = cum_gates.shape[2]
    width_a = query_a.shape[1] // heads
    width_b = query_b.shape[1] // heads
    group_size = lax.axis_size("sp")
    narrow = lax.axis_size("tp")
    here = lax.axis_index("sp")
    offset = here * rows
    gates_all = gathered_copies(cum_gates, "sp", 0)
    queries_a = query_a.reshape(rows, heads, width_a)
    queries_b = query_b.reshape(rows, heads, width_b)
    blocks = [(queries_a, queries_b, offset + jnp.arange(rows, dtype=jnp.int32), cum_gates)]
    initial = tuple(
        (
            (
                empty_state(block[2].shape[0], heads, width_a),
                empty_state(block[2].shape[0], heads, width_b),
            )
            for block in blocks
        )
    )
    start = jnp.int32(0)
    piece_key_a, piece_value_a, piece_key_b, piece_value_b = side_by_side(
        (
            key_a.reshape(rows, heads, width_a),
            value_a.reshape(rows, heads, width_a),
            key_b.reshape(rows, heads, width_b),
            value_b.reshape(rows, heads, width_b),
        ),
        "sp",
        0,
        2,
    )
    item_count = piece_key_a.shape[0]
    key_pos = jnp.arange(item_count, dtype=jnp.int32)
    updated = []
    for state, (block_a, block_b, position, block_gate) in zip(initial, blocks):

        def compute(current):
            mask = key_pos[None, :] <= position[:, None]
            return (
                update_state(
                    current[0],
                    block_a,
                    piece_key_a,
                    piece_value_a,
                    block_gate[:, 0, :],
                    gates_all[:, 0, :],
                    mask,
                    width_a,
                ),
                update_state(
                    current[1],
                    block_b,
                    piece_key_b,
                    piece_value_b,
                    block_gate[:, 1, :],
                    gates_all[:, 1, :],
                    mask,
                    width_b,
                ),
            )

        updated.append(lax.cond(start <= position[-1], compute, lambda current: current, state))
    folded = tuple(updated)
    attn_a = finish(folded[0][0])
    attn_b = finish(folded[0][1])
    proj = summed_on_arrival(
        (
            jnp.dot(attn_a, out_a, preferred_element_type=jnp.float32)
            + jnp.dot(attn_b, out_b, preferred_element_type=jnp.float32)
        ).astype(jnp.bfloat16),
        "tp",
        0,
    ).astype(jnp.bfloat16)
    post = rms_scale(proj.astype(jnp.float32), post_gain.astype(jnp.float32))
    mid_stream = (residual_in.astype(jnp.float32) + post).astype(jnp.bfloat16)
    normed = rms_scale(mid_stream.astype(jnp.float32), pre_gain.astype(jnp.float32)).astype(
        jnp.bfloat16
    )
    selected_count = expert_ids.shape[1]
    columns = normed.shape[1] // narrow
    slots = rows * selected_count * 5 // (4 * group_size)
    flat_experts = expert_ids.reshape(-1)
    onehot = (flat_experts[:, None] == jnp.arange(group_size, dtype=jnp.int32)[None, :]).astype(
        jnp.int32
    )
    rank = jnp.sum((jnp.cumsum(onehot, axis=0) - onehot) * onehot, axis=1)
    target = flat_experts * slots + rank
    owner = jnp.arange(rows * selected_count, dtype=jnp.int32) // selected_count
    table = jnp.full((group_size * slots,), -1, jnp.int32).at[target].set(owner)
    live = table >= 0
    source = jnp.maximum(table, 0)
    weighting = jnp.sum(
        expert_weights[:, :, None]
        * (
            target.reshape(rows, selected_count)[:, :, None]
            == jnp.arange(group_size * slots, dtype=jnp.int32)[None, None, :]
        ),
        axis=1,
    )
    column_rows = lax.all_to_all(normed, "tp", split_axis=1, concat_axis=0, tiled=True)
    outgoing = jnp.where(live[:, None], column_rows[source], jnp.zeros((), jnp.bfloat16))
    outgoing = outgoing.reshape(group_size, slots, columns)
    arrived = lax.all_to_all(outgoing, "sp", split_axis=0, concat_axis=0, tiled=True)
    flat = arrived.reshape(-1, columns)
    piece = gathered_copies(flat, "tp", 1)
    gate_rows = w_gate[0]
    up_rows = w_up[0]
    gate = jnp.dot(piece, gate_rows, preferred_element_type=jnp.float32)
    upward = jnp.dot(piece, up_rows, preferred_element_type=jnp.float32)
    hidden_rows = (jax.nn.silu(gate) * upward).astype(jnp.bfloat16)
    hidden = hidden_rows.reshape(arrived.shape[0], arrived.shape[1], -1)
    flat_hidden = hidden.reshape(-1, hidden.shape[2])
    down_cols = w_down[0]
    summed = summed_on_arrival(
        lax.dot_general(
            down_cols, flat_hidden, (((0,), (1,)), ((), ())), preferred_element_type=jnp.float32
        ).astype(jnp.bfloat16),
        "tp",
        0,
    )
    returned = lax.all_to_all(
        summed.astype(jnp.bfloat16).reshape(columns, group_size, slots),
        "sp",
        split_axis=1,
        concat_axis=1,
        tiled=True,
    )
    mixture_cols = jnp.einsum(
        "te,ce->tc", weighting, returned.reshape(columns, group_size * slots).astype(jnp.float32)
    )
    mixture = lax.all_to_all(
        mixture_cols.astype(jnp.bfloat16), "tp", split_axis=0, concat_axis=1, tiled=True
    ).astype(mixture_cols.dtype)
    return (mid_stream.astype(jnp.float32) + mixture).astype(jnp.bfloat16)


def solution(mesh):
    placed = (
        P(("sp", "tp"), None),
        P("sp", "tp"),
        P("sp", "tp"),
        P("sp", "tp"),
        P("sp", "tp"),
        P("sp", "tp"),
        P("sp", "tp"),
        P("sp", None, "tp"),
        P("tp", None),
        P("tp", None),
        P(),
        P(),
        P("sp", None),
        P("sp", None),
        P("sp", None, "tp"),
        P("sp", None, "tp"),
        P("sp", "tp", None),
    )
    return jax.shard_map(
        per_device, mesh=mesh, in_specs=placed, out_specs=P(("sp", "tp"), None), check_vma=False
    )
```

profile of v0, /device:TPU:1, one launch (start us, length us, event | category | flops | bytes accessed | tf_op | source)
XLA Modules:
  0.0 315.7 jit_solution(2174957318187156323)
XLA Ops:
  6.5 1.0 copy.60
  7.5 0.9 copy.59
  8.4 1.7 pad_maximum_fusion
  11.4 16.7 %all-to-all-start = ((f32[32,256,2,1]{1,2,3,0:T(2,128)}), f32[32,256,2,1]{1,2,3,0:T(2,128)S(1)}, u32[]{:S(2)}, u32[]{:S(2)}) async-start(f32[32,256,2,1]{1,2,3,0:T(2,128)} %broadcast_in_dim.39), calls=%async_computation | async-start | bytes 131072 | tf_op jit(solution)/shard_map/all_to_all | solution.py:18
  31.3 1.2 reduce-window.6
  33.7 7.5 %all-to-all-done = f32[32,256,2,1]{1,2,3,0:T(2,128)S(1)} async-done(((f32[32,256,2,1]{1,2,3,0:T(2,128)}), f32[32,256,2,1]{1,2,3,0:T(2,128)S(1)}, u32[]{:S(2)}, u32[]{:S(2)}) %all-to-all-start) | async-done | bytes 65568 | tf_op jit(solution)/shard_map/all_to_all | solution.py:18
  41.2 51.2 %all-gather.2.cloned.1.call-done = bf16[8192,1,384]{2,0,1:T(8,128)(2,1)} async-done(((bf16[256,1,384]{2,0,1:T(8,128)(2,1)}), bf16[8192,1,384]{2,0,1:T(8,128)(2,1)}) %all-gather.2.cloned.1.call-update) | async-done | bytes 6291472 | tf_op jit(solution)/shard_map/all_gather | solution.py:31
  92.4 25.4 %conditional.1 = (f32[1,256]{1,0:T(1,128)S(1)}, f32[1,256,64]{1,2,0:T(8,128)S(1)}, f32[1,256]{1,0:T(1,128)S(1)}, f32[1,256,128]{2,1,0:T(8,128)S(1)}) conditional(s32[]{:T(128)} %bitcast.13, () %tuple.13, (s32[8192]{0:T(1024)S(1)}, s32[256]{0:T(256)S(1)}, bf16[8192,1,384]{2,0,1:T(8,128)(2,1)}, bf16[256,64]{0,1:T(8,128)(2,1)}, f32[256,2,1]{0,2,1:T(1,128)}, ...), branch_computations={%region_0.0_spmd, %region_1.6_spmd} | conditional | flops 1665138176 | bytes 103798896 | solution.py:161
  93.3 8.6 %copy.61 = bf16[8192,1,384]{0,2,1:T(8,128)(2,1)} copy(bf16[8192,1,384]{2,0,1:T(8,128)(2,1)} %get-tuple-element.71) | data formatting | bytes 12582912 | tf_op jit(solution)/shard_map
  101.9 2.7 fusion.2
  105.0 3.5 %fusion.6 = (f32[256]{0:T(256)S(1)}, f32[256]{0:T(256)S(1)}, f32[256,8192]{1,0:T(8,128)S(1)}) fusion(s32[8192]{0:T(1024)S(1)} %get-tuple-element.29, s32[256]{0:T(256)S(1)} %get-tuple-element.30, f32[256,8192]{1,0:T(8,128)S(1)} %fusion.2, f32[8192]{0:T(1024)S(1)} %bitcast.123, f32[256]{0:T(256)S(1)} %bitcast.132, bf16[256,128]{1,0:T(8,128)(2,1)S(1)} %copy-done.9, ...), kind=kOutput, calls=%fused_computation.14 | convolution fusion | flops 553647616 | bytes 19009536 | tf_op jit(solution)/shard_map/cond/branch_1_fun/rhd,khd->hrk/dot_general | solution.py:59
  108.5 3.7 %fusion.9 = (f32[256]{0:T(256)S(1)}, f32[256]{0:T(256)S(1)}) fusion(f32[256,8192]{1,0:T(8,128)S(1)} %get-tuple-element.86, f32[256]{0:T(256)S(1)} %get-tuple-element.87, s32[8192]{0:T(1024)S(1)} %get-tuple-element.29, s32[256]{0:T(256)S(1)} %get-tuple-element.30, f32[256,8192]{1,0:T(8,128)S(1)} %fusion.2, f32[256]{0:T(256)S(1)} %get-tuple-element.88), kind=kLoop, calls=%fused_computation.17 | loop fusion | flops 14679552 | bytes 16815104 | tf_op jit(solution)/shard_map/cond/branch_1_fun/reduce_sum | solution.py:65
  112.2 3.1 fusion.25
  115.3 2.3 fusion.20
  118.3 1.5 fusion.30
  119.8 6.4 %all-to-all-start.1 = ((bf16[16,16,2048]{2,1,0:T(8,128)(2,1)}), bf16[16,16,2048]{2,1,0:T(8,128)(2,1)S(1)}, u32[]{:S(2)}, u32[]{:S(2)}) async-start(bf16[16,16,2048]{2,1,0:T(8,128)(2,1)} %bitcast.22), calls=%async_computation.1 | async-start | bytes 2097152 | tf_op jit(solution)/shard_map/all_to_all | solution.py:41
  126.4 2.4 scatter_custom_fusion
  129.0 13.7 %all-to-all-done.1 = bf16[16,16,2048]{2,1,0:T(8,128)(2,1)S(1)} async-done(((bf16[16,16,2048]{2,1,0:T(8,128)(2,1)}), bf16[16,16,2048]{2,1,0:T(8,128)(2,1)S(1)}, u32[]{:S(2)}, u32[]{:S(2)}) %all-to-all-start.1) | async-done | bytes 1048608 | tf_op jit(solution)/shard_map/all_to_all | solution.py:41
  143.9 4.5 %all-to-all-start.2 = ((bf16[16,16,128]{2,0,1:T(8,128)(2,1)}), bf16[16,16,128]{2,0,1:T(8,128)(2,1)S(1)}, u32[]{:S(2)}, u32[]{:S(2)}) async-start(bf16[16,16,128]{2,0,1:T(8,128)(2,1)} %copy_bitcast_fusion.1), calls=%async_computation.2 | async-start | bytes 131072 | tf_op jit(solution)/shard_map/all_to_all | solution.py:199
  148.4 6.5 %all-to-all-done.2 = bf16[16,16,128]{2,0,1:T(8,128)(2,1)S(1)} async-done(((bf16[16,16,128]{2,0,1:T(8,128)(2,1)}), bf16[16,16,128]{2,0,1:T(8,128)(2,1)S(1)}, u32[]{:S(2)}, u32[]{:S(2)}) %all-to-all-start.2) | async-done | bytes 65568 | tf_op jit(solution)/shard_map/all_to_all | solution.py:199
  154.9 2.0 gather_fusion
  157.2 28.4 %all_to_all.62 = bf16[32,20,128]{2,1,0:T(8,128)(2,1)S(1)} all-to-all(bf16[32,20,128]{2,1,0:T(8,128)(2,1)S(1)} %broadcast_select_fusion), channel_id=1, replica_groups=mesh['sp'=32,'tp'=16] {'sp'}, dimensions={0} | all-to-all | bytes 327680 | tf_op jit(solution)/shard_map/all_to_all | solution.py:202
  186.1 35.6 %all_to_all.63 = bf16[16,640,128]{1,2,0:T(8,128)(2,1)S(1)} all-to-all(bf16[16,640,128]{1,2,0:T(8,128)(2,1)S(1)} %broadcast_in_dim.64), channel_id=1, replica_groups=mesh['sp'=32,'tp'=16] {'tp'}, dimensions={0} | all-to-all | bytes 5242880 | tf_op jit(solution)/shard_map/all_to_all | solution.py:18
  221.7 1.5 copy-done.2
  223.2 2.1 fusion.35
  225.3 6.1 %fusion.31 = bf16[80,16,8,128]{3,2,1,0:T(8,128)(2,1)} fusion(bf16[1,256,2048]{2,1,0:T(8,128)(2,1)S(1)} %copy-done, bf16[640,2048]{0,1:T(8,128)(2,1)} %bitcast.115, bf16[1,2048,256]{2,1,0:T(8,128)(2,1)S(1)} %copy-done.8, f32[640,256]{1,0:T(8,128)S(1)} %fusion.35), kind=kOutput, calls=%fused_computation.38 | convolution fusion | flops 1344471040 | bytes 7995392 | tf_op jit(solution)/shard_map/dot_general | solution.py:214
  231.4 2.4 copy.84
  233.9 36.2 %all_to_all.64 = bf16[16,128,640]{1,2,0:T(8,128)(2,1)} all-to-all(bf16[16,128,640]{1,2,0:T(8,128)(2,1)S(1)} %bitcast.113), channel_id=1, replica_groups=mesh['sp'=32,'tp'=16] {'tp'}, dimensions={0} | all-to-all | bytes 5242880 | tf_op jit(solution)/shard_map/all_to_all | solution.py:41
  270.0 2.1 reduce_sum.93
  272.9 6.6 %all-to-all-start.6 = ((bf16[128,32,20]{0,2,1:T(8,128)(2,1)}), bf16[128,32,20]{0,2,1:T(8,128)(2,1)S(1)}, u32[]{:S(2)}, u32[]{:S(2)}) async-start(bf16[128,32,20]{0,2,1:T(8,128)(2,1)} %reshape.221), calls=%async_computation.6 | async-start | bytes 393216 | tf_op jit(solution)/shard_map/all_to_all | solution.py:220
  279.8 18.6 %all-to-all-done.6 = bf16[128,32,20]{0,2,1:T(8,128)(2,1)S(1)} async-done(((bf16[128,32,20]{0,2,1:T(8,128)(2,1)}), bf16[128,32,20]{0,2,1:T(8,128)(2,1)S(1)}, u32[]{:S(2)}, u32[]{:S(2)}) %all-to-all-start.6) | async-done | bytes 163872 | tf_op jit(solution)/shard_map/all_to_all | solution.py:220
  298.8 9.5 %all_to_all.65 = bf16[16,16,128]{2,1,0:T(8,128)(2,1)S(1)} all-to-all(bf16[16,16,128]{2,1,0:T(8,128)(2,1)S(1)} %bitcast.117), channel_id=1, replica_groups=mesh['sp'=32,'tp'=16] {'tp'}, dimensions={0} | all-to-all | bytes 131072 | tf_op jit(solution)/shard_map/all_to_all | solution.py:230
  (66 shorter events, 10.9 us)
Async XLA Ops:
  6.5 218.7 %copy-start = (bf16[1,256,2048]{2,1,0:T(8,128)(2,1)S(1)}, bf16[1,256,2048]{2,1,0:T(8,128)(2,1)}, u32[]{:S(2)}) copy-start(bf16[1,256,2048]{2,1,0:T(8,128)(2,1)} %param.35) | copy-start | bytes 3145732
  6.5 85.9 %all-gather.2.cloned.1.call-start = ((), (), s32[]{:S(2)}) async-start(), calls=%async_computation.8 | async-start | bytes 6488064 | tf_op jit(solution)/shard_map/all_gather | solution.py:31
  11.4 29.8 %all-to-all-start = ((f32[32,256,2,1]{1,2,3,0:T(2,128)}), f32[32,256,2,1]{1,2,3,0:T(2,128)S(1)}, u32[]{:S(2)}, u32[]{:S(2)}) async-start(f32[32,256,2,1]{1,2,3,0:T(2,128)} %broadcast_in_dim.39), calls=%async_computation | async-start | bytes 131072 | tf_op jit(solution)/shard_map/all_to_all | solution.py:18
  92.4 25.4 %copy-start.3 = (bf16[128,2048]{1,0:T(8,128)(2,1)S(1)}, bf16[128,2048]{1,0:T(8,128)(2,1)}, u32[]{:S(2)}) copy-start(bf16[128,2048]{1,0:T(8,128)(2,1)} %param.28) | copy-start | bytes 1572868
  92.4 25.9 %copy-start.4 = (bf16[64,2048]{1,0:T(8,128)(2,1)S(1)}, bf16[64,2048]{1,0:T(8,128)(2,1)}, u32[]{:S(2)}) copy-start(bf16[64,2048]{1,0:T(8,128)(2,1)} %param.27) | copy-start | bytes 786436
  92.4 9.5 %copy-start.6 = (bf16[256,64]{0,1:T(8,128)(2,1)S(1)}, bf16[256,64]{0,1:T(8,128)(2,1)}, u32[]{:S(2)}) copy-start(bf16[256,64]{0,1:T(8,128)(2,1)} %get-tuple-element.72) | copy-start | bytes 98308 | tf_op jit(solution)/shard_map/cond
  93.3 11.3 %copy-start.9 = (bf16[256,128]{1,0:T(8,128)(2,1)S(1)}, bf16[256,128]{1,0:T(8,128)(2,1)}, u32[]{:S(2)}) copy-start(bf16[256,128]{1,0:T(8,128)(2,1)} %get-tuple-element.47) | copy-start | bytes 196612 | tf_op jit(solution)/shard_map/cond
  101.9 3.1 copy-start.1
  117.8 25.2 %copy-start.5 = (bf16[16,2048]{1,0:T(8,128)(2,1)S(1)}, bf16[16,2048]{1,0:T(8,128)(2,1)}, u32[]{:S(2)}) copy-start(bf16[16,2048]{1,0:T(8,128)(2,1)} %param.19) | copy-start | bytes 196612
  119.8 22.9 %all-to-all-start.1 = ((bf16[16,16,2048]{2,1,0:T(8,128)(2,1)}), bf16[16,16,2048]{2,1,0:T(8,128)(2,1)S(1)}, u32[]{:S(2)}, u32[]{:S(2)}) async-start(bf16[16,16,2048]{2,1,0:T(8,128)(2,1)} %bitcast.22), calls=%async_computation.1 | async-start | bytes 2097152 | tf_op jit(solution)/shard_map/all_to_all | solution.py:41
  143.9 11.0 %all-to-all-start.2 = ((bf16[16,16,128]{2,0,1:T(8,128)(2,1)}), bf16[16,16,128]{2,0,1:T(8,128)(2,1)S(1)}, u32[]{:S(2)}, u32[]{:S(2)}) async-start(bf16[16,16,128]{2,0,1:T(8,128)(2,1)} %copy_bitcast_fusion.1), calls=%async_computation.2 | async-start | bytes 131072 | tf_op jit(solution)/shard_map/all_to_all | solution.py:199
  156.9 68.4 %copy-start.8 = (bf16[1,2048,256]{2,1,0:T(8,128)(2,1)S(1)}, bf16[1,2048,256]{2,1,0:T(8,128)(2,1)}, u32[]{:S(2)}) copy-start(bf16[1,2048,256]{2,1,0:T(8,128)(2,1)} %param.34) | copy-start | bytes 3145732
  221.7 1.5 copy-start.2
  231.4 48.2 %copy-start.7 = (f32[256,2]{0,1:T(2,128)S(1)}, f32[256,2]{0,1:T(2,128)}, u32[]{:S(2)}) copy-start(f32[256,2]{0,1:T(2,128)} %param.32) | copy-start | bytes 6148
  272.9 25.6 %all-to-all-start.6 = ((bf16[128,32,20]{0,2,1:T(8,128)(2,1)}), bf16[128,32,20]{0,2,1:T(8,128)(2,1)S(1)}, u32[]{:S(2)}, u32[]{:S(2)}) async-start(bf16[128,32,20]{0,2,1:T(8,128)(2,1)} %reshape.221), calls=%async_computation.6 | async-start | bytes 393216 | tf_op jit(solution)/shard_map/all_to_all | solution.py:220
Sparse Core Ops, SparseCore 0:
  10.2 82.1 all-gather.1
where the time goes:
time: 317 us; the launch traced here: 316 us
  blocking collectives  110 us (35%)
  waiting for transfers between devices  97.6 us (31%)
  starting transfers between devices  34.3 us (11%)
  local copies, waits for them, and re-layouts  25.1 us (8%)
  matrix products  22 us (7%)
  between operations  14.3 us (5%)
  other arithmetic  12.5 us (4%)
    all_gather x1, waiting for transfers between devices, side_by_side(): lax.all_gather(both, axis, axis=dim, tiled=True)  51.2 us
    all_to_all x1, blocking collectives, summed_on_arrival(): lax.all_to_all(blocks, axis, split_axis=0, concat_axis=0, tiled=True)  36.2 us
    all_to_all x1, blocking collectives, from_everyone(): return lax.all_to_all(copies, axis, split_axis=0, concat_axis=0, tiled=True)  35.6 us
    all_to_all x1, blocking collectives, per_device(): lax.all_to_all(outgoing, 'sp', split_axis=0, concat_axis=0, tiled=True)  28.4 us
    all_to_all x1, waiting for transfers between devices, per_device(): lax.all_to_all(summed.astype(jnp.bfloat16).reshape(columns, group_size, s...  18.6 us
    all_to_all x1, starting transfers between devices, from_everyone(): return lax.all_to_all(copies, axis, split_axis=0, concat_axis=0, tiled=True)  16.7 us
    all_to_all x1, waiting for transfers between devices, summed_on_arrival(): lax.all_to_all(blocks, axis, split_axis=0, concat_axis=0, tiled=True)  13.7 us
    all_to_all x1, blocking collectives, per_device(): lax.all_to_all(mixture_cols.astype(jnp.bfloat16), 'tp', split_axis=0, con...  9.46 us
  transfers between devices with their start and end apart: 5, of which 5 were waited for; matrix products, arithmetic and copies ran while one was open for 3% of the time, Pallas kernels for 0%

commit v1 on v0

--- a/solution.py
+++ b/solution.py
@@ -1,10 +1,230 @@
+import functools
+
 import jax
 import jax.numpy as jnp
 from jax import lax
+from jax.experimental import pallas as pl
+from jax.experimental.pallas import tpu as pltpu
 from jax.sharding import PartitionSpec as P
 
 eps_norm = 1e-06
 big_neg = -1e30
+log2e = 1.4426950408889634
+MESH = pl.DeviceIdType.MESH
+VM = pl.BlockSpec(memory_space=pltpu.VMEM)
+f32, bf16 = jnp.float32, jnp.bfloat16
+
+
+def nt_dot(a, b):
+    return lax.dot_general(a, b, (((1,), (1,)), ((), ())), preferred_element_type=f32)
+
+
+def attend_kernel(
+    group, q_a, k_a, v_a, q_b, k_b, v_b, gates, w_a, w_b, part,
+    kv_a, kv_k, kv_v, kv_g, qa, high_a, tot_a, acc_a, high_b, tot_b, acc_b,
+    ring_send, ring_recv, mate_send, mate_recv,
+):
+    rows = q_b.shape[0]
+    da = q_a.shape[0]
+    db = q_b.shape[1]
+    chips = group // 2
+    half = chips // 2
+    me = lax.axis_index("sp")
+    z, core = me // 2, lax.rem(me, 2)
+    right, left = lax.rem(me + 2, group), lax.rem(me + group - 2, group)
+    mate = me + 1 - 2 * core
+    barrier = pltpu.get_barrier_semaphore()
+    for peer in (right, left, mate):
+        pl.semaphore_signal(barrier, inc=1, device_id={"sp": peer}, device_id_type=MESH)
+    kv_a[me, :da, :] = k_a[...]
+    kv_a[me, da:, :] = v_a[...]
+    kv_k[me] = k_b[...]
+    kv_v[me] = v_b[...]
+    kv_g[me] = gates[...]
+    qa[...] = q_a[...].astype(f32).T.astype(bf16)
+    for high, tot, acc in ((high_a, tot_a, acc_a), (high_b, tot_b, acc_b)):
+        high[...] = jnp.full_like(high, big_neg)
+        tot[...] = jnp.zeros_like(tot)
+        acc[...] = jnp.zeros_like(acc)
+    pl.semaphore_wait(barrier, 3)
+
+    bufs = (kv_g, kv_a, kv_k, kv_v)
+
+    def hop(way, k, i, blk):
+        return pltpu.make_async_remote_copy(
+            src_ref=bufs[i].at[blk], dst_ref=bufs[i].at[blk],
+            send_sem=ring_send.at[way, k, i], recv_sem=ring_recv.at[way, k, i],
+            device_id={"sp": (right, left)[way]}, device_id_type=MESH,
+        )
+
+    def across(way, k, i, blk):
+        return pltpu.make_async_remote_copy(
+            src_ref=bufs[i].at[blk], dst_ref=bufs[i].at[blk],
+            send_sem=mate_send.at[way, k, i], recv_sem=mate_recv.at[way, k, i],
+            device_id={"sp": mate}, device_id_type=MESH,
+        )
+
+    def block_of(way, k, base):
+        shift = (group - 2 * k) if way == 0 else 2 * k
+        return lax.rem(base + shift, group)
+
+    for i in range(4):
+        hop(0, 1, i, me).start()
+        hop(1, 1, i, me).start()
+        across(0, 0, i, me).start()
+
+    def update(blocks, mask, query, keys, values, scale, which, high, tot, acc):
+        scores = []
+        for blk in blocks:
+            s = keys(query, blk) * (scale * log2e) - kv_g[blk, which] * log2e
+            if mask is not None:
+                s = jnp.where(mask, s, big_neg)
+            scores.append(s)
+        top = jnp.max(functools.reduce(jnp.maximum, scores), axis=1, keepdims=True)
+        old = high[...]
+        new = jnp.maximum(old, top)
+        fade = jnp.exp2(old - new)
+        high[...] = new
+        weights = [jnp.exp2(s - new) for s in scores]
+        tot[...] = tot[...] * fade + jnp.sum(functools.reduce(jnp.add, weights), axis=1, keepdims=True)
+        mixed = functools.reduce(jnp.add, [values(w.astype(bf16), blk) for w, blk in zip(weights, blocks)])
+        acc[...] = acc[...] * fade + mixed
+
+    def fold(blocks, mask=None):
+        update(
+            blocks, mask, qa[...],
+            lambda q, blk: jnp.dot(q, kv_a[blk, :da, :], preferred_element_type=f32),
+            lambda w, blk: nt_dot(w, kv_a[blk, da:, :]),
+            da ** -0.5, 0, high_a, tot_a, acc_a,
+        )
+        update(
+            blocks, mask, q_b[...],
+            lambda q, blk: nt_dot(q, kv_k[blk]),
+            lambda w, blk: jnp.dot(w, kv_v[blk], preferred_element_type=f32),
+            db ** -0.5, 1, high_b, tot_b, acc_b,
+        )
+
+    row = lax.broadcasted_iota(jnp.int32, (rows, rows), 0)
+    col = lax.broadcasted_iota(jnp.int32, (rows, rows), 1)
+    fold([me], col <= row)
+    for i in range(4):
+        across(0, 0, i, mate).wait_recv()
+
+    @pl.when(core == 1)
+    def _():
+        fold([mate])
+
+    def needed(way, k):
+        return (z >= k) if way == 0 else (z + k >= chips)
+
+    def unit(way, k):
+        for i in range(4):
+            across(way, k, i, block_of(way, k, mate)).wait_recv()
+
+        @pl.when(needed(way, k))
+        def _():
+            fold([block_of(way, k, me), block_of(way, k, mate)])
+
+    def take(way, k, i, onward):
+        blk = block_of(way, k, me)
+        hop(way, k, i, blk).wait_recv()
+        if onward is True:
+            hop(way, k + 1, i, blk).start()
+        elif onward is not None:
+            @pl.when(onward)
+            def _():
+                hop(way, k + 1, i, blk).start()
+        across(way, k, i, blk).start()
+
+    last_way = (0, 0, 0, 1)
+
+    def step(k, carry):
+        for i in range(2):
+            for way in range(2):
+                take(way, k, i, True if last_way[i] == way else k < half - 1)
+
+        @pl.when(k > 1)
+        def _():
+            unit(0, k - 1)
+
+        for way in range(2):
+            take(way, k, 2, True if last_way[2] == way else k < half - 1)
+
+        @pl.when(k > 1)
+        def _():
+            unit(1, k - 1)
+
+        for way in range(2):
+            take(way, k, 3, True if last_way[3] == way else k < half - 1)
+        return carry
+
+    lax.fori_loop(1, half, step, 0)
+    unit(0, half - 1)
+    unit(1, half - 1)
+    for i in range(4):
+        way = last_way[i]
+        blk = block_of(way, half, me)
+        hop(way, half, i, blk).wait_recv()
+        across(0, half, i, blk).start()
+    unit(0, half)
+
+    out_a = (acc_a[...] / tot_a[...]).astype(bf16)
+    out_b = (acc_b[...] / tot_b[...]).astype(bf16)
+    wide = min(512, part.shape[1])
+    for at in range(0, part.shape[1], wide):
+        cols = slice(at, at + wide)
+        part[:, cols] = (
+            jnp.dot(out_a, w_a[:, cols], preferred_element_type=f32)
+            + jnp.dot(out_b, w_b[:, cols], preferred_element_type=f32)
+        ).astype(bf16)
+
+    def drain(k, carry):
+        for i in range(4):
+            for way in range(2):
+                hop(way, k, i, me).wait_send()
+                across(way, k, i, me).wait_send()
+        return carry
+
+    lax.fori_loop(1, half, drain, 0)
+    for i in range(4):
+        hop(last_way[i], half, i, me).wait_send()
+        across(0, half, i, me).wait_send()
+        across(0, 0, i, me).wait_send()
+
+
+def attend(query_a, key_a, value_a, query_b, key_b, value_b, cum_gates, out_a, out_b):
+    rows, da = query_a.shape
+    db = query_b.shape[1]
+    group = lax.axis_size("sp")
+    half = group // 4
+    return pl.pallas_call(
+        functools.partial(attend_kernel, group),
+        out_shape=jax.ShapeDtypeStruct((rows, out_a.shape[1]), bf16),
+        in_specs=[VM] * 9,
+        out_specs=VM,
+        scratch_shapes=[
+            pltpu.VMEM((group, 2 * da, rows), bf16),
+            pltpu.VMEM((group, rows, db), bf16),
+            pltpu.VMEM((group, rows, db), bf16),
+            pltpu.VMEM((group, 2, 1, rows), f32),
+            pltpu.VMEM((rows, da), bf16),
+            pltpu.VMEM((rows, 1), f32),
+            pltpu.VMEM((rows, 1), f32),
+            pltpu.VMEM((rows, da), f32),
+            pltpu.VMEM((rows, 1), f32),
+            pltpu.VMEM((rows, 1), f32),
+            pltpu.VMEM((rows, db), f32),
+            pltpu.SemaphoreType.DMA((2, half + 1, 4)),
+            pltpu.SemaphoreType.DMA((2, half + 1, 4)),
+            pltpu.SemaphoreType.DMA((2, half + 1, 4)),
+            pltpu.SemaphoreType.DMA((2, half + 1, 4)),
+        ],
+        compiler_params=pltpu.CompilerParams(collective_id=1, has_side_effects=True),
+        name="attend",
+    )(
+        query_a.T, key_a.T, value_a.T, query_b, key_b, value_b,
+        cum_gates.transpose(1, 2, 0), out_a, out_b,
+    )
 
 
 def joined_along(blocks, dim):
@@ -103,70 +323,11 @@
     narrow = lax.axis_size("tp")
     here = lax.axis_index("sp")
     offset = here * rows
-    gates_all = gathered_copies(cum_gates, "sp", 0)
-    queries_a = query_a.reshape(rows, heads, width_a)
-    queries_b = query_b.reshape(rows, heads, width_b)
-    blocks = [(queries_a, queries_b, offset + jnp.arange(rows, dtype=jnp.int32), cum_gates)]
-    initial = tuple(
-        (
-            (
-                empty_state(block[2].shape[0], heads, width_a),
-                empty_state(block[2].shape[0], heads, width_b),
-            )
-            for block in blocks
-        )
-    )
-    start = jnp.int32(0)
-    piece_key_a, piece_value_a, piece_key_b, piece_value_b = side_by_side(
-        (
-            key_a.reshape(rows, heads, width_a),
-            value_a.reshape(rows, heads, width_a),
-            key_b.reshape(rows, heads, width_b),
-            value_b.reshape(rows, heads, width_b),
-        ),
-        "sp",
-        0,
-        2,
-    )
-    item_count = piece_key_a.shape[0]
-    key_pos = jnp.arange(item_count, dtype=jnp.int32)
-    updated = []
-    for state, (block_a, block_b, position, block_gate) in zip(initial, blocks):
-
-        def compute(current):
-            mask = key_pos[None, :] <= position[:, None]
-            return (
-                update_state(
-                    current[0],
-                    block_a,
-                    piece_key_a,
-                    piece_value_a,
-                    block_gate[:, 0, :],
-                    gates_all[:, 0, :],
-                    mask,
-                    width_a,
-                ),
-                update_state(
-                    current[1],
-                    block_b,
-                    piece_key_b,
-                    piece_value_b,
-                    block_gate[:, 1, :],
-                    gates_all[:, 1, :],
-                    mask,
-                    width_b,
-                ),
-            )
-
-        updated.append(lax.cond(start <= position[-1], compute, lambda current: current, state))
-    folded = tuple(updated)
-    attn_a = finish(folded[0][0])
-    attn_b = finish(folded[0][1])
+    part = attend(
+        query_a, key_a, value_a, query_b, key_b, value_b, cum_gates, out_a, out_b
+    )
     proj = summed_on_arrival(
-        (
-            jnp.dot(attn_a, out_a, preferred_element_type=jnp.float32)
-            + jnp.dot(attn_b, out_b, preferred_element_type=jnp.float32)
-        ).astype(jnp.bfloat16),
+        part,
         "tp",
         0,
     ).astype(jnp.bfloat16)

time: 317 us -> 247 us (0.78)
  waiting for transfers between devices: 97.6 us -> 40.2 us
  Pallas kernels: 0 us -> 53.9 us
  starting transfers between devices: 34.3 us -> 17 us
  matrix products: 22 us -> 7.21 us
  between operations: 14.3 us -> 0.28 us
  local copies, waits for them, and re-layouts: 25.1 us -> 11.1 us
  other arithmetic: 12.5 us -> 5.79 us
    pallas_call x0 -> x1, Pallas kernels: none -> 53.9 us  [attend(): pl.pallas_call(functools.partial(attend_kernel, group), out_shape=jax.Sha...]
    all_gather x1 -> x0, waiting for transfers between devices: 51.2 us -> none  [side_by_side(): lax.all_gather(both, axis, axis=dim, tiled=True)]
    all_to_all x1 -> x0, starting transfers between devices: 16.7 us -> none  [from_everyone(): return lax.all_to_all(copies, axis, split_axis=0, concat_axis=0, tiled=True)]
    dot_general x6 -> x0, matrix products: 13.5 us -> none  [the longest x2 6.17 us: update_state(): jnp.einsum('rhd,khd->hrk', query, key_rows, preferred_element_type=jnp.fl...]
    another operation x2 -> x1, local copies, waits for them, and re-layouts: 8.63 us -> 0.01 us
    all_to_all x1 -> x0, waiting for transfers between devices: 7.51 us -> none  [from_everyone(): return lax.all_to_all(copies, axis, split_axis=0, concat_axis=0, tiled=True)]
    reduce_sum x1 -> x0, other arithmetic: 3.7 us -> none  [update_state(): total = jnp.sum(expo, axis=2)]
  transfers between devices with their start and end apart: 5 -> 3, of which waited for: 5 -> 3; matrix products, arithmetic and copies ran while one was open for 3% -> 2% of each run, Pallas kernels for 0% -> 0%
where the time goes in v1:
time: 247 us; the launch traced here: 246 us
  blocking collectives  110 us (45%)
  Pallas kernels  53.9 us (22%)
  waiting for transfers between devices  40.2 us (16%)
  starting transfers between devices  17 us (7%)
  local copies, waits for them, and re-layouts  11.1 us (4%)
  matrix products  7.21 us (3%)
  other arithmetic  5.79 us (2%)
    pallas_call x1, Pallas kernels, attend(): pl.pallas_call(functools.partial(attend_kernel, group), out_shape=jax.Sha...  53.9 us
    all_to_all x1, blocking collectives, summed_on_arrival(): lax.all_to_all(blocks, axis, split_axis=0, concat_axis=0, tiled=True)  36.2 us
    all_to_all x1, blocking collectives, from_everyone(): return lax.all_to_all(copies, axis, split_axis=0, concat_axis=0, tiled=True)  35.7 us
    all_to_all x1, blocking collectives, per_device(): lax.all_to_all(outgoing, 'sp', split_axis=0, concat_axis=0, tiled=True)  29.1 us
    all_to_all x1, waiting for transfers between devices, per_device(): lax.all_to_all(summed.astype(jnp.bfloat16).reshape(columns, group_size, s...  18.6 us
    all_to_all x1, waiting for transfers between devices, summed_on_arrival(): lax.all_to_all(blocks, axis, split_axis=0, concat_axis=0, tiled=True)  15.1 us
    all_to_all x1, blocking collectives, per_device(): lax.all_to_all(mixture_cols.astype(jnp.bfloat16), 'tp', split_axis=0, con...  9.46 us
    all_to_all x1, starting transfers between devices, summed_on_arrival(): lax.all_to_all(blocks, axis, split_axis=0, concat_axis=0, tiled=True)  6.9 us
  transfers between devices with their start and end apart: 3, of which 3 were waited for; matrix products, arithmetic and copies ran while one was open for 2% of the time, Pallas kernels for 0%

profile of v1, /device:TPU:1, one launch (start us, length us, event | category | flops | bytes accessed | tf_op | source)
XLA Modules:
  0.0 246.0 jit_solution(17041982732790717504)
XLA Ops:
  0.0 53.9 %attend.1 = bf16[256,2048]{1,0:T(8,128)(2,1)} custom-call(bf16[64,256]{1,0:T(8,128)(2,1)} %bitcast.75, bf16[64,256]{1,0:T(8,128)(2,1)} %bitcast.76, bf16[64,256]{1,0:T(8,128)(2,1)} %bitcast.77, bf16[256,128]{1,0:T(8,128)(2,1)} %q_b.1, bf16[256,128]{1,0:T(8,128)(2,1)} %k_b.1, bf16[256,128]{1,0:T(8,128)(2,1)} %v_b.1, f32[2,1,256]{2,1,0:T(1,128)} %bitcast.79, ...), custom_call_target="tpu_custom_call" | custom-call | tf_op jit(solution)/shard_map/attend/pallas_call | solution.py:200
  54.0 6.9 %all-to-all-start = ((bf16[16,16,2048]{2,1,0:T(8,128)(2,1)}), bf16[16,16,2048]{2,1,0:T(8,128)(2,1)S(1)}, u32[]{:S(2)}, u32[]{:S(2)}) async-start(bf16[16,16,2048]{2,1,0:T(8,128)(2,1)} %bitcast.71), calls=%async_computation | async-start | bytes 2097152 | tf_op jit(solution)/shard_map/all_to_all | solution.py:261
  61.0 0.1 eq.42
  61.3 1.2 reduce-window.6
  62.5 0.2 slice_reduce_fusion
  63.3 2.4 scatter_custom_fusion
  65.8 15.1 %all-to-all-done = bf16[16,16,2048]{2,1,0:T(8,128)(2,1)S(1)} async-done(((bf16[16,16,2048]{2,1,0:T(8,128)(2,1)}), bf16[16,16,2048]{2,1,0:T(8,128)(2,1)S(1)}, u32[]{:S(2)}, u32[]{:S(2)}) %all-to-all-start) | async-done | bytes 1048608 | tf_op jit(solution)/shard_map/all_to_all | solution.py:261
  81.0 0.1 reduce_sum.64
  81.3 0.2 fusion.13
  81.5 0.7 copy_bitcast_fusion.1
  82.2 3.5 %all-to-all-start.1 = ((bf16[16,16,128]{2,0,1:T(8,128)(2,1)}), bf16[16,16,128]{2,0,1:T(8,128)(2,1)S(1)}, u32[]{:S(2)}, u32[]{:S(2)}) async-start(bf16[16,16,128]{2,0,1:T(8,128)(2,1)} %copy_bitcast_fusion.1), calls=%async_computation.1 | async-start | bytes 131072 | tf_op jit(solution)/shard_map/all_to_all | solution.py:360
  85.8 6.4 %all-to-all-done.1 = bf16[16,16,128]{2,0,1:T(8,128)(2,1)S(1)} async-done(((bf16[16,16,128]{2,0,1:T(8,128)(2,1)}), bf16[16,16,128]{2,0,1:T(8,128)(2,1)S(1)}, u32[]{:S(2)}, u32[]{:S(2)}) %all-to-all-start.1) | async-done | bytes 65568 | tf_op jit(solution)/shard_map/all_to_all | solution.py:360
  92.2 2.0 gather_fusion
  94.2 0.2 broadcast_select_fusion
  94.4 29.1 %all_to_all.57 = bf16[32,20,128]{2,1,0:T(8,128)(2,1)S(1)} all-to-all(bf16[32,20,128]{2,1,0:T(8,128)(2,1)S(1)} %broadcast_select_fusion), channel_id=1, replica_groups=mesh['sp'=32,'tp'=16] {'sp'}, dimensions={0} | all-to-all | bytes 327680 | tf_op jit(solution)/shard_map/all_to_all | solution.py:363
  123.5 0.2 copy.45
  123.7 0.3 broadcast_in_dim.37
  124.0 35.7 %all_to_all.58 = bf16[16,640,128]{1,2,0:T(8,128)(2,1)S(1)} all-to-all(bf16[16,640,128]{1,2,0:T(8,128)(2,1)S(1)} %broadcast_in_dim.37), channel_id=1, replica_groups=mesh['sp'=32,'tp'=16] {'tp'}, dimensions={0} | all-to-all | bytes 5242880 | tf_op jit(solution)/shard_map/all_to_all | solution.py:238
  159.8 1.5 copy-done.1
  161.3 0.9 fusion.4
  162.2 0.3 copy-done.8
  162.5 6.1 %fusion = bf16[80,16,8,128]{3,2,1,0:T(8,128)(2,1)} fusion(bf16[1,256,2048]{2,1,0:T(8,128)(2,1)S(1)} %copy-done, bf16[640,2048]{0,1:T(8,128)(2,1)} %bitcast.73, bf16[1,2048,256]{2,1,0:T(8,128)(2,1)S(1)} %copy-done.8, f32[640,256]{1,0:T(8,128)S(1)} %fusion.4), kind=kOutput, calls=%fused_computation.4 | convolution fusion | flops 1344471040 | bytes 7995392 | tf_op jit(solution)/shard_map/dot_general | solution.py:375
  168.6 2.4 copy.56
  171.0 36.2 %all_to_all.59 = bf16[16,128,640]{1,2,0:T(8,128)(2,1)} all-to-all(bf16[16,128,640]{1,2,0:T(8,128)(2,1)S(1)} %bitcast.70), channel_id=1, replica_groups=mesh['sp'=32,'tp'=16] {'tp'}, dimensions={0} | all-to-all | bytes 5242880 | tf_op jit(solution)/shard_map/all_to_all | solution.py:261
  207.2 2.1 reduce_sum.71
  209.3 0.7 reshape.110
  210.0 6.6 %all-to-all-start.5 = ((bf16[128,32,20]{0,2,1:T(8,128)(2,1)}), bf16[128,32,20]{0,2,1:T(8,128)(2,1)S(1)}, u32[]{:S(2)}, u32[]{:S(2)}) async-start(bf16[128,32,20]{0,2,1:T(8,128)(2,1)} %reshape.110), calls=%async_computation.5 | async-start | bytes 393216 | tf_op jit(solution)/shard_map/all_to_all | solution.py:381
  216.8 0.2 select_reduce_fusion
  217.0 18.6 %all-to-all-done.5 = bf16[128,32,20]{0,2,1:T(8,128)(2,1)S(1)} async-done(((bf16[128,32,20]{0,2,1:T(8,128)(2,1)}), bf16[128,32,20]{0,2,1:T(8,128)(2,1)S(1)}, u32[]{:S(2)}, u32[]{:S(2)}) %all-to-all-start.5) | async-done | bytes 163872 | tf_op jit(solution)/shard_map/all_to_all | solution.py:381
  235.7 0.2 fusion.30
  235.9 9.5 %all_to_all.60 = bf16[16,16,128]{2,1,0:T(8,128)(2,1)S(1)} all-to-all(bf16[16,16,128]{2,1,0:T(8,128)(2,1)S(1)} %bitcast.74), channel_id=1, replica_groups=mesh['sp'=32,'tp'=16] {'tp'}, dimensions={0} | all-to-all | bytes 131072 | tf_op jit(solution)/shard_map/all_to_all | solution.py:391
  245.4 0.6 fusion.16
  (40 shorter events, 1.2 us)
Async XLA Ops:
  0.0 162.2 %copy-start = (bf16[1,256,2048]{2,1,0:T(8,128)(2,1)S(1)}, bf16[1,256,2048]{2,1,0:T(8,128)(2,1)}, u32[]{:S(2)}) copy-start(bf16[1,256,2048]{2,1,0:T(8,128)(2,1)} %param.33) | copy-start | bytes 3145732
  0.0 60.9 %copy-start.5 = (s32[256,2]{0,1:T(2,128)S(1)}, s32[256,2]{0,1:T(2,128)}, u32[]{:S(2)}) copy-start(s32[256,2]{0,1:T(2,128)} %param.29) | copy-start | bytes 6148
  0.0 63.2 %copy-start.3 = (bf16[2048]{0:T(1024)(128)(2,1)S(1)}, bf16[2048]{0:T(1024)(128)(2,1)}, u32[]{:S(2)}) copy-start(bf16[2048]{0:T(1024)(128)(2,1)} %param.27) | copy-start | bytes 12292
  0.0 63.2 %copy-start.4 = (bf16[2048]{0:T(1024)(128)(2,1)S(1)}, bf16[2048]{0:T(1024)(128)(2,1)}, u32[]{:S(2)}) copy-start(bf16[2048]{0:T(1024)(128)(2,1)} %param.28) | copy-start | bytes 12292
  54.0 27.3 %copy-start.2 = (bf16[16,2048]{1,0:T(8,128)(2,1)S(1)}, bf16[16,2048]{1,0:T(8,128)(2,1)}, u32[]{:S(2)}) copy-start(bf16[16,2048]{1,0:T(8,128)(2,1)} %param.17) | copy-start | bytes 196612
  54.0 27.0 %all-to-all-start = ((bf16[16,16,2048]{2,1,0:T(8,128)(2,1)}), bf16[16,16,2048]{2,1,0:T(8,128)(2,1)S(1)}, u32[]{:S(2)}, u32[]{:S(2)}) async-start(bf16[16,16,2048]{2,1,0:T(8,128)(2,1)} %bitcast.71), calls=%async_computation | async-start | bytes 2097152 | tf_op jit(solution)/shard_map/all_to_all | solution.py:261
  82.2 10.0 %all-to-all-start.1 = ((bf16[16,16,128]{2,0,1:T(8,128)(2,1)}), bf16[16,16,128]{2,0,1:T(8,128)(2,1)S(1)}, u32[]{:S(2)}, u32[]{:S(2)}) async-start(bf16[16,16,128]{2,0,1:T(8,128)(2,1)} %copy_bitcast_fusion.1), calls=%async_computation.1 | async-start | bytes 131072 | tf_op jit(solution)/shard_map/all_to_all | solution.py:360
  124.0 37.3 %copy-start.7 = (bf16[1,2048,256]{2,1,0:T(8,128)(2,1)S(1)}, bf16[1,2048,256]{2,1,0:T(8,128)(2,1)}, u32[]{:S(2)}) copy-start(bf16[1,2048,256]{2,1,0:T(8,128)(2,1)} %param.31) | copy-start | bytes 3145732
  159.8 1.5 copy-start.1
  161.3 1.2 copy-start.8
  207.2 9.6 %copy-start.6 = (f32[256,2]{0,1:T(2,128)S(1)}, f32[256,2]{0,1:T(2,128)}, u32[]{:S(2)}) copy-start(f32[256,2]{0,1:T(2,128)} %param.30) | copy-start | bytes 6148
  210.0 25.6 %all-to-all-start.5 = ((bf16[128,32,20]{0,2,1:T(8,128)(2,1)}), bf16[128,32,20]{0,2,1:T(8,128)(2,1)S(1)}, u32[]{:S(2)}, u32[]{:S(2)}) async-start(bf16[128,32,20]{0,2,1:T(8,128)(2,1)} %reshape.110), calls=%async_computation.5 | async-start | bytes 393216 | tf_op jit(solution)/shard_map/all_to_all | solution.py:381
